TPU v7x, 32 devices: a whole 2x2x4 slice. The times are simulated.
32 devices in a mesh: fs: 16 (over z, y, x), tp: 2 (over core).
Axes of the slice: x: 2, y: 2, z: 4, core: 2. Of those that a mesh axis runs over, the one named last changes fastest.
Arguments:
- fwd_input: bfloat16 [2048, 2048], P('fs'), may hold values from -6 to 6
- saved_input: bfloat16 [2048, 2048], P('fs'), may hold values from -6 to 6
- out_cotangent: bfloat16 [2048, 2048], P('fs'), may hold values from -6 to 6
- up_weight: bfloat16 [2048, 4096], P('fs', 'tp'), may hold values from -0.125 to 0.125
- down_weight: bfloat16 [4096, 2048], P('tp', 'fs'), may hold values from -0.09375 to 0.09375
- up_grad_sum: float32 [2048, 4096], P('fs', 'tp'), may hold values from -6 to 6
Outputs:
- layer_out: bfloat16 [2048, 2048], P('fs')
- input_grad: bfloat16 [2048, 2048], P('fs')
- up_grad_out: float32 [2048, 4096], P('fs', 'tp')
All inputs are finite; a program needn't handle non-finite values.
Results may differ from a plain program's by a relative error of at most 0.013.
Values may be sent and summed in bfloat16 or wider, within the bound.
A program may use at most 128 MiB of HBM per device.

v0:
```python
import jax
import jax.numpy as jnp
from jax import lax
from jax.sharding import PartitionSpec as P


def per_device(fwd_input, saved_input, out_cotangent, up_weight, down_weight, up_grad_sum):
    row_count = fwd_input.shape[0]
    stacked = jnp.concatenate([fwd_input, saved_input], axis=0)
    up_whole = lax.all_gather(up_weight, "fs", axis=0, tiled=True)
    down_whole = lax.all_gather(down_weight, "fs", axis=1, tiled=True)
    pre_both = jnp.dot(stacked, up_whole, preferred_element_type=jnp.float32)
    pre_fwd = pre_both[:row_count]
    pre_bwd = pre_both[row_count:]
    positive = jnp.maximum(pre_fwd, 0.0)
    hidden = (positive * positive).astype(jnp.bfloat16)
    out_part = jnp.dot(hidden, down_whole, preferred_element_type=jnp.float32)
    layer_out = lax.psum(out_part.astype(jnp.bfloat16), "tp")
    d_hidden = lax.dot_general(
        out_cotangent, down_whole, (((1,), (1,)), ((), ())), preferred_element_type=jnp.float32
    )
    d_pre = (d_hidden * 2.0 * jnp.maximum(pre_bwd, 0.0)).astype(jnp.bfloat16)
    in_part = lax.dot_general(
        d_pre, up_whole, (((1,), (1,)), ((), ())), preferred_element_type=jnp.float32
    )
    input_grad = lax.psum(in_part.astype(jnp.bfloat16), "tp")
    grad_part = lax.psum_scatter(
        lax.dot_general(
            saved_input, d_pre, (((0,), (0,)), ((), ())), preferred_element_type=jnp.float32
        ),
        "fs",
        scatter_dimension=0,
        tiled=True,
    )
    grad_scale = float(row_count * lax.axis_size("fs")) ** (-0.5)
    return (layer_out, input_grad, up_grad_sum + grad_part * grad_scale)


def solution(mesh):
    placed = (
        P("fs", None),
        P("fs", None),
        P("fs", None),
        P("fs", "tp"),
        P("tp", "fs"),
        P("fs", "tp"),
    )
    return jax.shard_map(
        per_device,
        mesh=mesh,
        in_specs=placed,
        out_specs=(P("fs", None), P("fs", None), P("fs", "tp")),
        check_vma=False,
    )
```

profile of v0, /device:TPU:0, one launch (start us, length us, event | category | flops | bytes accessed | tf_op | source)
XLA Modules:
  0.0 666.1 jit_solution(1798604370416390500)
XLA Ops:
  7.2 0.0 copy-start
  7.2 0.0 all-gather.3.cloned.1.call-start
  7.2 0.7 all-gather.3.cloned.1.call-update
  7.9 0.0 all-gather.5.cloned.1.call-start
  8.0 0.7 all-gather.5.cloned.1.call-update
  8.7 0.0 reduce-scatter.2.cloned.1.call-start
  8.7 117.1 %all-gather.3.cloned.1.call-done = bf16[2048,2048]{1,0:T(8,128)(2,1)} async-done(((bf16[128,2048]{1,0:T(8,128)(2,1)}), bf16[2048,2048]{1,0:T(8,128)(2,1)}) %all-gather.3.cloned.1.call-update) | async-done | bytes 8388624 | tf_op jit(solution)/shard_map/all_gather | solution.py:10
  125.8 6.0 fusion.4
  131.9 136.7 %all-gather.5.cloned.1.call-done = bf16[2048,2048]{1,0:T(8,128)(2,1)} async-done(((bf16[2048,128]{1,0:T(8,128)(2,1)}), bf16[2048,2048]{1,0:T(8,128)(2,1)}) %all-gather.5.cloned.1.call-update) | async-done | bytes 8388624 | tf_op jit(solution)/shard_map/all_gather | solution.py:11
  268.6 0.0 copy-done
  268.6 0.0 copy-start.1
  268.6 6.3 fusion.1
  274.9 0.0 copy-done.1
  274.9 8.1 %convolution_bitcast_fusion = f32[2048,2048]{0,1:T(8,128)} fusion(bf16[128,2048]{1,0:T(8,128)(2,1)S(1)} %fusion.1, bf16[128,2048]{1,0:T(8,128)(2,1)S(1)} %copy-done.1), kind=kOutput, calls=%fused_computation | convolution fusion | flops 1073741824 | bytes 17825792 | tf_op jit(solution)/shard_map/dot_general | solution.py:28
  283.0 0.0 reduce-scatter.2.cloned.1.call-update
  283.0 0.0 all-reduce.3.cloned.1.call-start
  283.1 7.1 %convolution_convert_fusion = bf16[128,2048]{1,0:T(8,128)(2,1)} fusion(bf16[128,2048]{1,0:T(8,128)(2,1)S(1)} %fusion.1, bf16[2048,2048]{1,0:T(8,128)(2,1)} %all-gather.3.cloned.1.call-done), kind=kOutput, calls=%fused_computation.3 | convolution fusion | flops 1074003968 | bytes 9437184 | tf_op jit(solution)/shard_map/dot_general | solution.py:23
  290.2 5.4 convolution_convert_fusion.1
  295.6 0.0 all-reduce.3.cloned.1.call-update
  295.6 1.6 copy.9
  297.2 330.6 %reduce-scatter.2.cloned.1.call-done = f32[128,2048]{0,1:T(8,128)} async-done(((f32[2048,2048]{0,1:T(8,128)}), f32[128,2048]{0,1:T(8,128)}) %reduce-scatter.2.cloned.1.call-update) | async-done | bytes 1048592 | tf_op jit(solution)/shard_map/reduce_scatter | solution.py:27
  627.8 1.3 multiply_add_fusion
  629.2 1.3 copy.10
  630.5 25.3 %all-reduce.3.cloned.1.call-done = (bf16[128,2048]{1,0:T(8,128)(2,1)}, bf16[128,2048]{1,0:T(8,128)(2,1)}) async-done(((bf16[128,2048]{1,0:T(8,128)(2,1)}, bf16[128,2048]{1,0:T(8,128)(2,1)}), (bf16[128,2048]{1,0:T(8,128)(2,1)}, bf16[128,2048]{1,0:T(8,128)(2,1)})) %all-reduce.3.cloned.1.call-update) | async-done | bytes 1048592 | tf_op jit(solution)/shard_map/psum | solution.py:18
  655.8 1.9 copy.13
  657.7 1.9 copy.14
Async XLA Ops:
  7.2 261.4 %copy-start = (bf16[128,2048]{1,0:T(8,128)(2,1)S(1)}, bf16[128,2048]{1,0:T(8,128)(2,1)}, u32[]{:S(2)}) copy-start(bf16[128,2048]{1,0:T(8,128)(2,1)} %param.8) | copy-start | bytes 1572868
  7.2 118.6 %all-gather.3.cloned.1.call-start = ((), (), s32[]{:S(2)}) async-start(), calls=%async_computation.1 | async-start | bytes 8912896 | tf_op jit(solution)/shard_map/all_gather | solution.py:10
  7.9 260.6 %all-gather.5.cloned.1.call-start = ((), (), s32[]{:S(2)}) async-start(), calls=%async_computation.2 | async-start | bytes 8912896 | tf_op jit(solution)/shard_map/all_gather | solution.py:11
  8.7 619.1 %reduce-scatter.2.cloned.1.call-start = ((), (), s32[]{:S(2)}) async-start(), calls=%async_computation.3 | async-start | bytes 17825792 | tf_op jit(solution)/shard_map/reduce_scatter | solution.py:27
  268.6 6.3 copy-start.1
  283.0 372.7 %all-reduce.3.cloned.1.call-start = ((), (), s32[]{:S(2)}) async-start(), calls=%async_computation.4 | async-start | bytes 2097152 | tf_op jit(solution)/shard_map/psum | solution.py:18
Sparse Core Ops, SparseCore 0:
  10.8 115.0 all-gather.2
  128.5 139.9 all-gather.4
  283.2 344.5 reduce-scatter.1
  630.6 25.1 all-reduce.2
where the time goes:
time: 666 us
  waiting for transfers between devices  611 us (92%)
  matrix products  33 us (5%)
  between operations  13.8 us (2%)
    reduce_scatter x1, waiting for transfers between devices, per_device(): lax.psum_scatter(lax.dot_general(saved_input, d_pre, (((0,), (0,)), ((),...  331 us
    all_gather x1, waiting for transfers between devices, per_device(): down_whole = lax.all_gather(down_weight, 'fs', axis=1, tiled=True)  137 us
    all_gather x1, waiting for transfers between devices, per_device(): up_whole = lax.all_gather(up_weight, 'fs', axis=0, tiled=True)  117 us
    psum x1, waiting for transfers between devices, per_device(): layer_out = lax.psum(out_part.astype(jnp.bfloat16), 'tp')  25.3 us
  transfers between devices with their start and end apart: 4, of which 4 were waited for; matrix products, arithmetic and copies ran while one was open for 3% of the time, Pallas kernels for 0%

commit v1 on v0

--- a/solution.py
+++ b/solution.py
@@ -8,7 +8,7 @@
     row_count = fwd_input.shape[0]
     stacked = jnp.concatenate([fwd_input, saved_input], axis=0)
     up_whole = lax.all_gather(up_weight, "fs", axis=0, tiled=True)
-    down_whole = lax.all_gather(down_weight, "fs", axis=1, tiled=True)
+    down_whole = jnp.concatenate(lax.all_gather(down_weight, "fs"), axis=1)
     pre_both = jnp.dot(stacked, up_whole, preferred_element_type=jnp.float32)
     pre_fwd = pre_both[:row_count]
     pre_bwd = pre_both[row_count:]

time: 666 us -> 638 us (0.958)
  waiting for transfers between devices: 611 us -> 574 us
  local copies, waits for them, and re-layouts: 6.63 us -> 19.1 us
    all_gather x1, waiting for transfers between devices: 137 us -> 117 us  [per_device(): down_whole = jnp.concatenate(lax.all_gather(down_weight, 'fs'), axis=1)]
    all_gather x1, waiting for transfers between devices: 117 us -> 101 us  [per_device(): up_whole = lax.all_gather(up_weight, 'fs', axis=0, tiled=True)]
    reshape x0 -> x1, local copies, waits for them, and re-layouts: none -> 12.4 us  [per_device(): down_whole = jnp.concatenate(lax.all_gather(down_weight, 'fs'), axis=1)]
  transfers between devices with their start and end apart: 4 -> 4, of which waited for: 4 -> 4; matrix products, arithmetic and copies ran while one was open for 3% -> 5% of each run, Pallas kernels for 0% -> 0%
where the time goes in v1:
time: 638 us
  waiting for transfers between devices  574 us (90%)
  matrix products  29.7 us (5%)
  local copies, waits for them, and re-layouts  19.1 us (3%)
  between operations  13.8 us (2%)
    reduce_scatter x1, waiting for transfers between devices, per_device(): lax.psum_scatter(lax.dot_general(saved_input, d_pre, (((0,), (0,)), ((),...  329 us
    all_gather x1, waiting for transfers between devices, per_device(): down_whole = jnp.concatenate(lax.all_gather(down_weight, 'fs'), axis=1)  117 us
    all_gather x1, waiting for transfers between devices, per_device(): up_whole = lax.all_gather(up_weight, 'fs', axis=0, tiled=True)  101 us
    psum x1, waiting for transfers between devices, per_device(): layer_out = lax.psum(out_part.astype(jnp.bfloat16), 'tp')  25.3 us
  transfers between devices with their start and end apart: 4, of which 4 were waited for; matrix products, arithmetic and copies ran while one was open for 5% of the time, Pallas kernels for 0%

profile of v1, /device:TPU:0, one launch (start us, length us, event | category | flops | bytes accessed | tf_op | source)
XLA Modules:
  0.0 637.8 jit_solution(6117836198412460235)
XLA Ops:
  7.2 0.0 copy-start
  7.2 0.0 all-gather.6.cloned.1.call-start
  7.2 0.7 all-gather.6.cloned.1.call-update
  7.9 0.0 all-gather.4.cloned.1.call-start
  8.0 0.7 all-gather.4.cloned.1.call-update
  8.7 0.0 reduce-scatter.2.cloned.1.call-start
  8.7 117.1 %all-gather.6.cloned.1.call-done = bf16[32768,128]{1,0:T(8,128)(2,1)} async-done(((bf16[2048,128]{1,0:T(8,128)(2,1)}), bf16[32768,128]{1,0:T(8,128)(2,1)}) %all-gather.6.cloned.1.call-update) | async-done | bytes 8388624 | tf_op jit(solution)/shard_map/all_gather | solution.py:11
  125.8 0.0 copy-start.2
  125.8 12.4 %copy.13 = bf16[2048,16,128]{0,2,1:T(8,128)(2,1)} copy(bf16[2048,16,128]{2,0,1:T(8,128)(2,1)} %bitcast.16) | data formatting | bytes 16777216 | tf_op jit(solution)/shard_map/reshape | solution.py:11
  138.2 100.9 %all-gather.4.cloned.1.call-done = bf16[2048,2048]{1,0:T(8,128)(2,1)} async-done(((bf16[128,2048]{1,0:T(8,128)(2,1)}), bf16[2048,2048]{1,0:T(8,128)(2,1)}) %all-gather.4.cloned.1.call-update) | async-done | bytes 8388624 | tf_op jit(solution)/shard_map/all_gather | solution.py:10
  239.1 0.0 copy-done.2
  239.1 0.0 copy-start.1
  239.1 6.0 fusion.4
  245.1 0.0 copy-start.3
  245.1 0.0 copy-done
  245.1 0.0 copy-done.1
  245.1 1.4 fusion.1
  246.6 0.0 copy-done.3
  246.6 8.1 %convolution_bitcast_fusion = f32[2048,2048]{0,1:T(8,128)} fusion(bf16[128,2048]{1,0:T(8,128)(2,1)S(1)} %fusion.1, bf16[128,2048]{1,0:T(8,128)(2,1)S(1)} %copy-done.3), kind=kOutput, calls=%fused_computation | convolution fusion | flops 1073741824 | bytes 17825792 | tf_op jit(solution)/shard_map/dot_general | solution.py:28
  254.7 0.0 reduce-scatter.2.cloned.1.call-update
  254.7 0.0 all-reduce.3.cloned.1.call-start
  254.8 7.1 %convolution_convert_fusion = bf16[128,2048]{1,0:T(8,128)(2,1)} fusion(bf16[128,2048]{1,0:T(8,128)(2,1)S(1)} %fusion.1, bf16[2048,2048]{1,0:T(8,128)(2,1)} %all-gather.4.cloned.1.call-done), kind=kOutput, calls=%fused_computation.3 | convolution fusion | flops 1074003968 | bytes 9437184 | tf_op jit(solution)/shard_map/dot_general | solution.py:23
  261.9 7.1 %convolution_convert_fusion.1 = bf16[128,2048]{1,0:T(8,128)(2,1)} fusion(bf16[2048,2048]{0,1:T(8,128)(2,1)} %bitcast.14, f32[256,2048]{1,0:T(8,128)S(1)} %fusion.4), kind=kOutput, calls=%fused_computation.4 | convolution fusion | flops 1074790400 | bytes 9961472 | tf_op jit(solution)/shard_map/dot_general | solution.py:17
  268.9 0.0 all-reduce.3.cloned.1.call-update
  268.9 1.6 copy.14
  270.5 328.9 %reduce-scatter.2.cloned.1.call-done = f32[128,2048]{0,1:T(8,128)} async-done(((f32[2048,2048]{0,1:T(8,128)}), f32[128,2048]{0,1:T(8,128)}) %reduce-scatter.2.cloned.1.call-update) | async-done | bytes 1048592 | tf_op jit(solution)/shard_map/reduce_scatter | solution.py:27
  599.5 1.3 multiply_add_fusion
  600.8 1.3 copy.15
  602.1 25.3 %all-reduce.3.cloned.1.call-done = (bf16[128,2048]{1,0:T(8,128)(2,1)}, bf16[128,2048]{1,0:T(8,128)(2,1)}) async-done(((bf16[128,2048]{1,0:T(8,128)(2,1)}, bf16[128,2048]{1,0:T(8,128)(2,1)}), (bf16[128,2048]{1,0:T(8,128)(2,1)}, bf16[128,2048]{1,0:T(8,128)(2,1)})) %all-reduce.3.cloned.1.call-update) | async-done | bytes 1048592 | tf_op jit(solution)/shard_map/psum | solution.py:18
  627.5 1.9 copy.18
  629.4 1.9 copy.19
Async XLA Ops:
  7.2 238.0 %copy-start = (bf16[128,2048]{1,0:T(8,128)(2,1)S(1)}, bf16[128,2048]{1,0:T(8,128)(2,1)}, u32[]{:S(2)}) copy-start(bf16[128,2048]{1,0:T(8,128)(2,1)} %param.8) | copy-start | bytes 1572868
  7.2 118.6 %all-gather.6.cloned.1.call-start = ((), (), s32[]{:S(2)}) async-start(), calls=%async_computation.3 | async-start | bytes 8912896 | tf_op jit(solution)/shard_map/all_gather | solution.py:11
  7.9 231.2 %all-gather.4.cloned.1.call-start = ((), (), s32[]{:S(2)}) async-start(), calls=%async_computation.1 | async-start | bytes 8912896 | tf_op jit(solution)/shard_map/all_gather | solution.py:10
  8.7 590.8 %reduce-scatter.2.cloned.1.call-start = ((), (), s32[]{:S(2)}) async-start(), calls=%async_computation.2 | async-start | bytes 17825792 | tf_op jit(solution)/shard_map/reduce_scatter | solution.py:27
  125.8 113.3 %copy-start.2 = (bf16[128,2048]{1,0:T(8,128)(2,1)S(1)}, bf16[128,2048]{1,0:T(8,128)(2,1)}, u32[]{:S(2)}) copy-start(bf16[128,2048]{1,0:T(8,128)(2,1)} %param.7) | copy-start | bytes 1572868
  239.1 6.0 copy-start.1
  245.1 1.5 copy-start.3
  254.7 372.7 %all-reduce.3.cloned.1.call-start = ((), (), s32[]{:S(2)}) async-start(), calls=%async_computation.4 | async-start | bytes 2097152 | tf_op jit(solution)/shard_map/psum | solution.py:18
Sparse Core Ops, SparseCore 0:
  10.8 115.0 all-gather.5
  128.6 110.4 all-gather.3
  254.9 344.5 reduce-scatter.1
  602.3 25.1 all-reduce.2
